TPU v7x, 32 devices: a whole 2x2x4 slice. The times are simulated.
32 devices in a mesh: sp: 4 (over z), dp: 8 (over y, x, core).
Axes of the slice: x: 2, y: 2, z: 4, core: 2. Of those that a mesh axis runs over, the one named last changes fastest.
Arguments:
- tokens: bfloat16 [8, 512, 2048], P('dp', 'sp'), may hold values from -6 to 6
- receptance_weight: bfloat16 [2048, 1024], P('dp'), may hold values from -0.125 to 0.125
- key_projection_weight: bfloat16 [2048, 1024], P('dp'), may hold values from -0.125 to 0.125
- value_projection_weight: bfloat16 [2048, 1024], P('dp'), may hold values from -0.125 to 0.125
- decay_down_weight: bfloat16 [2048, 256], P('dp'), may hold values from -0.125 to 0.125
- decay_up_weight: bfloat16 [2, 128, 1024], replicated, may hold values from -0.71875 to 0.71875
- decay_floor_level: float32 [2, 1024], replicated, may hold values from -10 to -2.25
- correction_rate_logit: float32 [2, 1024], P(None, 'sp'), may hold values from -4 to 4
- diagonal_address_factor: float32 [2, 1024], P(None, 'sp'), may hold values from -1 to 1
- head_norm_gain: float32 [1024], P('sp'), may hold values from 0.1 to 1.9
Outputs:
- mixed: bfloat16 [8, 512, 1024], P('dp', 'sp')
All inputs are finite; a program needn't handle non-finite values.
Results may differ from a plain program's by a relative error of at most 0.0056.
The roundings to bfloat16 on the way count: a program that leaves them out, or rounds other values in their place, can miss the bound.
Values may be sent and summed in bfloat16 or wider, within the bound.
A program may use at most 128 MiB of HBM per device.

v0:
```python
import math

import jax
import jax.numpy as jnp
from jax import lax
from jax.sharding import PartitionSpec as P

SUBSPACE_SIZE = 64


def contract(pattern, former, latter):
    return jnp.einsum(pattern, former, latter, precision=lax.Precision.HIGHEST)


def project_rows(totals, pieces, source):
    results = []
    for running, piece in zip(totals, pieces):
        results.append(jnp.dot(source, piece, preferred_element_type=jnp.float32))
    return tuple(results)


def both_ways(content_matrix_full):
    return jnp.stack([content_matrix_full, jnp.flip(content_matrix_full, 0)], 0)


def advance(state, pair):
    transfer_block, inject_block = pair
    later = contract("...ij,...jk->...ik", state, transfer_block) + inject_block
    return (later, state)


def per_device(
    tokens,
    receptance_weight,
    key_projection_weight,
    value_projection_weight,
    decay_down_weight,
    decay_up_weight,
    decay_floor_level,
    correction_rate_logit,
    diagonal_address_factor,
    head_norm_gain,
):
    depth = tokens.shape[2]
    source = tokens.reshape(-1, depth)
    row_count = source.shape[0]
    channels = receptance_weight.shape[1]
    low_width = decay_down_weight.shape[1]
    empty = jnp.zeros((row_count, channels), jnp.float32)
    initial = (empty, empty, empty, jnp.zeros((row_count, low_width), jnp.float32))
    sums = project_rows(
        initial,
        (
            lax.all_gather(receptance_weight, "dp", axis=0, tiled=True),
            lax.all_gather(key_projection_weight, "dp", axis=0, tiled=True),
            lax.all_gather(value_projection_weight, "dp", axis=0, tiled=True),
            lax.all_gather(decay_down_weight, "dp", axis=0, tiled=True),
        ),
        source,
    )
    receive = sums[0].astype(jnp.bfloat16)
    key_rows = sums[1].astype(jnp.bfloat16)
    value_rows = sums[2].astype(jnp.bfloat16)
    lowered = jnp.tanh(sums[3]).astype(jnp.bfloat16)
    rank = decay_up_weight.shape[1]
    forward_pre = (
        jnp.dot(lowered[:, :rank], decay_up_weight[0], preferred_element_type=jnp.float32)
        + decay_floor_level[0]
    ).astype(jnp.bfloat16)
    backward_pre = (
        jnp.dot(lowered[:, rank:], decay_up_weight[1], preferred_element_type=jnp.float32)
        + decay_floor_level[1]
    ).astype(jnp.bfloat16)
    moved = (
        lax.all_to_all(receive, "sp", split_axis=1, concat_axis=0, tiled=True),
        lax.all_to_all(key_rows, "sp", split_axis=1, concat_axis=0, tiled=True),
        lax.all_to_all(value_rows, "sp", split_axis=1, concat_axis=0, tiled=True),
        lax.all_to_all(forward_pre, "sp", split_axis=1, concat_axis=0, tiled=True),
        lax.all_to_all(backward_pre, "sp", split_axis=1, concat_axis=0, tiled=True),
    )
    length = moved[0].shape[0]
    local_channels = moved[0].shape[1]
    subspace_dimension = SUBSPACE_SIZE
    subspace_batches = local_channels // subspace_dimension
    span = math.gcd(length, 64)
    blocks = length // span

    def by_head(content_matrix_full):
        return content_matrix_full.astype(jnp.float32).reshape(
            length, subspace_batches, subspace_dimension
        )

    def to_blocks(content_matrix_full):
        return jnp.transpose(
            content_matrix_full.reshape(2, blocks, span, subspace_batches, subspace_dimension),
            (0, 3, 1, 2, 4),
        )

    gate_by_subspace = by_head(moved[0])
    address_by_subspace = by_head(moved[1])
    value_per_head = by_head(moved[2])
    amend_strength = jax.nn.sigmoid(correction_rate_logit).reshape(
        2, 1, subspace_batches, subspace_dimension
    )
    normed = address_by_subspace / jnp.sqrt(
        jnp.sum(address_by_subspace * address_by_subspace, -1, keepdims=True) + 1.0
    )
    decay_log = -math.exp(-0.5) * jax.nn.sigmoid(
        jnp.stack([by_head(moved[3]), jnp.flip(by_head(moved[4]), 0)], 0)
    )
    block_rate = jnp.transpose(amend_strength, (0, 2, 1, 3))[:, :, :, None, :]
    probe_matrix_full = to_blocks(both_ways(gate_by_subspace))
    content_matrix_full = to_blocks(both_ways(value_per_head))
    erasers = -to_blocks(both_ways(normed))
    writers = -erasers * block_rate
    rated_keys = to_blocks(both_ways(address_by_subspace)) * block_rate
    log_decay = to_blocks(decay_log)
    inclusive = jnp.cumsum(log_decay, axis=3)
    previous = inclusive - log_decay
    middle = inclusive[:, :, :, span // 2 : span // 2 + 1]
    final = inclusive[:, :, :, span - 1 : span]
    erase_query = erasers * jnp.exp(previous - middle)
    read_query = probe_matrix_full * jnp.exp(inclusive - middle)
    write_key = writers * jnp.exp(middle - inclusive)
    plain_key = rated_keys * jnp.exp(middle - inclusive)
    strict = jnp.tril(jnp.ones((span, span), jnp.bool_), -1)
    lower = jnp.tril(jnp.ones((span, span), jnp.bool_))
    erase_write = jnp.where(strict, contract("...tn,...jn->...tj", erase_query, write_key), 0.0)
    erase_plain = jnp.where(strict, contract("...tn,...jn->...tj", erase_query, plain_key), 0.0)
    read_write = jnp.where(lower, contract("...tn,...jn->...tj", read_query, write_key), 0.0)
    read_plain = jnp.where(lower, contract("...tn,...jn->...tj", read_query, plain_key), 0.0)
    identity = jnp.eye(span, dtype=jnp.float32)
    inverse = lax.linalg.triangular_solve(
        identity - erase_write,
        jnp.broadcast_to(identity, erase_write.shape),
        left_side=True,
        lower=True,
        unit_diagonal=True,
    )
    to_end = jnp.exp(final - inclusive)
    carried = contract("...jt,...jn->...tn", inverse, writers * to_end)
    start_erase = erasers * jnp.exp(previous)
    transfer = contract("...tm,...tn->...mn", start_erase, carried) + jnp.eye(
        subspace_dimension, dtype=jnp.float32
    ) * jnp.exp(final)
    inject = contract(
        "...tv,...tn->...vn",
        content_matrix_full,
        contract("...jt,...jn->...tn", erase_plain, carried) + rated_keys * to_end,
    )
    start_state = jnp.zeros(
        (2, subspace_batches, subspace_dimension, subspace_dimension), jnp.float32
    )
    _, entering = lax.scan(
        advance, start_state, (jnp.moveaxis(transfer, 2, 0), jnp.moveaxis(inject, 2, 0))
    )
    entering = jnp.moveaxis(entering, 0, 2)
    pulled = contract(
        "...tj,...jv->...tv",
        inverse,
        contract("...tk,...vk->...tv", start_erase, entering)
        + contract("...tj,...jv->...tv", erase_plain, content_matrix_full),
    )
    outputs = (
        contract("...tk,...vk->...tv", probe_matrix_full * jnp.exp(inclusive), entering)
        + contract("...tj,...jv->...tv", read_write, pulled)
        + contract("...tj,...jv->...tv", read_plain, content_matrix_full)
    )
    ordered = jnp.transpose(outputs, (0, 2, 3, 1, 4)).reshape(
        2, length, subspace_batches, subspace_dimension
    )
    ordered = jnp.stack([ordered[0], jnp.flip(ordered[1], 0)], 0)
    centred = ordered - jnp.mean(ordered, -1, keepdims=True)
    variance = jnp.mean(centred * centred, -1, keepdims=True)
    gain = head_norm_gain.reshape(1, 1, subspace_batches, subspace_dimension)
    normalized = centred * lax.rsqrt(variance + 0.00064) * gain
    diagonal_extra = diagonal_address_factor.reshape(2, 1, subspace_batches, subspace_dimension)
    diagonal_contribution = (
        jnp.sum(
            gate_by_subspace * address_by_subspace * amend_strength * diagonal_extra,
            -1,
            keepdims=True,
        )
        * value_per_head
    )
    mixed = (
        jnp.sum(normalized + diagonal_contribution, 0)
        .reshape(length, local_channels)
        .astype(jnp.bfloat16)
    )
    returned = lax.all_to_all(mixed, "sp", split_axis=0, concat_axis=1, tiled=True)
    return returned.reshape(1, row_count, channels)


def solution(mesh):
    in_specs = (
        P("dp", "sp", None),
        P("dp", None),
        P("dp", None),
        P("dp", None),
        P("dp", None),
        P(),
        P(),
        P(None, "sp"),
        P(None, "sp"),
        P("sp"),
    )
    out_specs = P("dp", "sp", None)
    return jax.shard_map(
        per_device, mesh=mesh, in_specs=in_specs, out_specs=out_specs, check_vma=False
    )
```

profile of v0, /device:TPU:0, one launch (start us, length us, event | category | flops | bytes accessed | tf_op | source)
XLA Modules:
  0.0 670.7 jit_solution(8530076982883730021)
XLA Ops:
  10.2 25.1 %all-gather.7.cloned.1.call-done = bf16[2048,256]{1,0:T(8,128)(2,1)} async-done(((bf16[256,256]{1,0:T(8,128)(2,1)}), bf16[2048,256]{1,0:T(8,128)(2,1)}) %all-gather.7.cloned.1.call-update) | async-done | bytes 1048592 | tf_op jit(solution)/shard_map/all_gather | solution.py:57
  38.0 4.6 all-to-all-start.2
  43.7 8.2 %all-to-all-done.2 = bf16[128,4,256]{0,2,1:T(8,128)(2,1)S(1)} async-done(((bf16[128,4,256]{0,2,1:T(8,128)(2,1)}), bf16[128,4,256]{0,2,1:T(8,128)(2,1)S(1)}, u32[]{:S(2)}, u32[]{:S(2)}) %all-to-all-start.2) | async-done | bytes 262176 | tf_op jit(solution)/shard_map/all_to_all | solution.py:79
  51.9 3.4 all-to-all-start.1
  57.7 4.6 all-to-all-done.1
  69.4 4.5 all-gather.9.cloned.1.call-done
  77.6 4.6 all-to-all-start.3
  82.8 29.5 %all-gather.11.cloned.1.call-done = bf16[2048,1024]{1,0:T(8,128)(2,1)} async-done(((bf16[256,1024]{1,0:T(8,128)(2,1)}), bf16[2048,1024]{1,0:T(8,128)(2,1)}) %all-gather.11.cloned.1.call-update) | async-done | bytes 4194320 | tf_op jit(solution)/shard_map/all_gather | solution.py:56
  112.4 2.9 convolution_convert_fusion
  116.1 4.6 all-to-all-start.4
  120.7 30.0 %all-gather.5.cloned.1.call-done = bf16[2048,1024]{1,0:T(8,128)(2,1)} async-done(((bf16[256,1024]{1,0:T(8,128)(2,1)}), bf16[2048,1024]{1,0:T(8,128)(2,1)}) %all-gather.5.cloned.1.call-update) | async-done | bytes 4194320 | tf_op jit(solution)/shard_map/all_gather | solution.py:54
  150.7 3.6 convolution_convert_fusion.2
  156.2 4.8 all-to-all-start
  180.5 3.4 rev.19
  195.0 7.6 %add_bitcast_fusion.1 = f32[2,4,8,1,64,64]{5,4,3,2,1,0:T(8,128)} fusion(f32[64,64]{1,0:T(8,128)S(1)} %copy-done.34, f32[64,64]{1,0:T(8,128)S(1)} %get-tuple-element.101, pred[64,64]{1,0:T(8,128)(4,1)S(1)} %get-tuple-element.100, f32[2,4,8,64,64]{4,2,3,1,0:T(8,128)S(1)} %fusion.17, f32[2,4,64]{2,1,0:T(4,128)S(1)} %mul.142, ...), kind=kOutput, calls=%fused_computation.47 | convolution fusion | flops 206045184 | bytes 4249600 | tf_op jit(solution)/shard_map/...tn,...jn->...tj/dot_general | solution.py:12
  202.6 316.2 %custom-call.3 = f32[2,4,8,1,64,64]{4,5,3,2,1,0:T(8,128)} custom-call(f32[2,4,8,1,64,64]{5,4,3,2,1,0:T(8,128)} %add_bitcast_fusion.1), custom_call_target="InvertDiagBlocksLowerTriangular" | custom-call | tf_op jit(solution)/shard_map/triangular_solve | solution.py:133
  518.7 6.4 fusion.14
  526.5 9.2 %fusion.77 = f32[2,4,8,64,64]{4,3,2,1,0:T(8,128)} fusion(f32[1,8,64,4,64]{4,2,1,3,0:T(8,128)} %bitcast.178, f32[1,8,64,4,64]{4,2,1,3,0:T(8,128)} %copy.201, f32[2,4,8,64,64]{4,2,3,1,0:T(8,128)S(1)} %fusion.17, f32[2,4,64]{2,1,0:T(4,128)S(1)} %mul.142, f32[2,4,8,64]{3,2,1,0:T(8,128)S(1)} %get-tuple-element.94, f32[1,8,64,4,64]{4,2,1,3,0:T(8,128)} %bitcast.181, ...), kind=kOutput, calls=%fused_computation.108 | convolution fusion | flops 204996608 | bytes 5261312 | tf_op jit(solution)/shard_map/...tn,...jn->...tj/dot_general | solution.py:12
  543.4 4.1 fusion.16
  547.5 3.6 fusion.36
  551.1 4.9 fusion.34
  556.1 4.4 fusion.42
  560.5 5.8 bitcast_add_fusion
  566.3 27.8 %while.13 = (s32[]{:T(128)}, f32[2,4,64,64]{2,3,1,0:T(8,128)S(1)}, f32[8,2,4,64,64]{3,4,2,1,0:T(8,128)}, f32[8,2,4,64,64]{4,3,0,2,1:T(8,128)}, f32[8,2,4,64,64]{4,3,0,2,1:T(8,128)}, /*index=5*/s32[]{:T(128)}, s32[]{:T(128)}) while((s32[]{:T(128)}, f32[2,4,64,64]{2,3,1,0:T(8,128)S(1)}, f32[8,2,4,64,64]{3,4,2,1,0:T(8,128)}, ...), condition=%wide.region_3.4_spmd.clone, body=%wide.region_2.3_spmd.clone.sunk | while | flops 25264132 | bytes 1836124 | solution.py:154
  594.0 7.4 %fusion.31 = f32[2,4,8,64,64]{4,3,2,1,0:T(8,128)} fusion(f32[1,8,64,4,64]{4,2,1,3,0:T(8,128)} %bitcast.182, f32[1,8,64,4,64]{4,2,1,3,0:T(8,128)} %copy-done.15, f32[2,4,8,64,64]{4,2,3,1,0:T(8,128)S(1)} %fusion.17, f32[1,8,64,4,64]{4,2,1,3,0:T(8,128)} %bitcast.189, f32[1,8,64,4,64]{4,2,1,3,0:T(8,128)} %copy.194, f32[8,2,4,64,64]{3,4,2,1,0:T(8,128)} %get-tuple-element.32), kind=kOutput, calls=%fused_computation.52 | convolution fusion | flops 203685888 | bytes 5242880 | tf_op jit(solution)/shard_map/...tk,...vk->...tv/dot_general | solution.py:12
  605.4 8.1 %fusion.75 = f32[2,4,8,64,64]{4,3,2,1,0:T(8,128)} fusion(f32[1,8,64,4,64]{4,2,1,3,0:T(8,128)} %bitcast.175, f32[1,8,64,4,64]{4,2,1,3,0:T(8,128)} %copy.188, f32[2,4,8,64,64]{4,2,3,1,0:T(8,128)S(1)} %fusion.17, f32[2,4,8,64]{3,2,1,0:T(8,128)S(1)} %get-tuple-element.94, f32[2,4,64]{2,1,0:T(4,128)S(1)} %mul.142, f32[1,8,64,4,64]{4,2,1,3,0:T(8,128)} %bitcast.183, ...), kind=kOutput, calls=%fused_computation.107 | convolution fusion | flops 203161600 | bytes 4212736 | tf_op jit(solution)/shard_map/...tn,...jn->...tj/dot_general | solution.py:12
  613.5 4.0 fusion.28
  617.5 6.0 fusion.74
  624.9 5.2 fusion.21
  633.0 3.6 add_bitcast_fusion
  637.8 6.8 %rev.24 = f32[512,4,64]{2,0,1:T(8,128)S(1)} reverse(f32[512,4,64]{2,0,1:T(8,128)} %bitcast.192), dimensions={0} | reverse | bytes 1048576 | tf_op jit(solution)/shard_map/jit(_flip)/rev | solution.py:172
  649.2 13.6 %all_to_all.78 = bf16[4,128,256]{1,2,0:T(8,128)(2,1)S(1)} all-to-all(bf16[4,128,256]{1,2,0:T(8,128)(2,1)S(1)} %copy.226), channel_id=1, replica_groups=mesh['sp'=4,'dp'=8] {'sp'}, dimensions={0} | all-to-all | bytes 524288 | tf_op jit(solution)/shard_map/all_to_all | solution.py:191
  (200 shorter events, 105.2 us)
Async XLA Ops:
  6.5 28.8 %copy-start = (bf16[1,128,2048]{2,1,0:T(8,128)(2,1)S(1)}, bf16[1,128,2048]{2,1,0:T(8,128)(2,1)}, u32[]{:S(2)}) copy-start(bf16[1,128,2048]{2,1,0:T(8,128)(2,1)} %param.12) | copy-start | bytes 1572868
  6.5 30.4 %copy-start.32 = (bf16[2,128,1024]{2,1,0:T(8,128)(2,1)S(1)}, bf16[2,128,1024]{2,1,0:T(8,128)(2,1)}, u32[]{:S(2)}) copy-start(bf16[2,128,1024]{2,1,0:T(8,128)(2,1)} %param.17) | copy-start | bytes 1572868
  6.5 28.8 %all-gather.7.cloned.1.call-start = ((), (), s32[]{:S(2)}) async-start(), calls=%async_computation.7 | async-start | bytes 1179648 | tf_op jit(solution)/shard_map/all_gather | solution.py:57
  7.3 66.6 %all-gather.9.cloned.1.call-start = ((), (), s32[]{:S(2)}) async-start(), calls=%async_computation.8 | async-start | bytes 4718592 | tf_op jit(solution)/shard_map/all_gather | solution.py:55
  8.0 34.6 %copy-start.36 = (f32[2,256]{1,0:T(2,128)S(1)}, f32[2,256]{1,0:T(2,128)}, u32[]{:S(2)}) copy-start(f32[2,256]{1,0:T(2,128)} %param.19) | copy-start | bytes 6148
  8.0 104.3 %all-gather.11.cloned.1.call-start = ((), (), s32[]{:S(2)}) async-start(), calls=%async_computation.9 | async-start | bytes 4718592 | tf_op jit(solution)/shard_map/all_gather | solution.py:56
  8.8 142.0 %all-gather.5.cloned.1.call-start = ((), (), s32[]{:S(2)}) async-start(), calls=%async_computation.6 | async-start | bytes 4718592 | tf_op jit(solution)/shard_map/all_gather | solution.py:54
  10.2 45.2 %copy-start.35 = (f32[2,256]{1,0:T(2,128)S(1)}, f32[2,256]{1,0:T(2,128)}, u32[]{:S(2)}) copy-start(f32[2,256]{1,0:T(2,128)} %param.20) | copy-start | bytes 6148
  10.2 45.3 %copy-start.37 = (f32[256]{0:T(256)S(1)}, f32[256]{0:T(256)}, u32[]{:S(2)}) copy-start(f32[256]{0:T(256)} %param.21) | copy-start | bytes 3076
  38.0 13.9 %all-to-all-start.2 = ((bf16[128,4,256]{0,2,1:T(8,128)(2,1)}), bf16[128,4,256]{0,2,1:T(8,128)(2,1)S(1)}, u32[]{:S(2)}, u32[]{:S(2)}) async-start(bf16[128,4,256]{0,2,1:T(8,128)(2,1)} %bitcast.11), calls=%async_computation.2 | async-start | bytes 524288 | tf_op jit(solution)/shard_map/all_to_all | solution.py:79
  51.9 10.4 %all-to-all-start.1 = ((bf16[128,4,256]{0,2,1:T(8,128)(2,1)}), bf16[128,4,256]{0,2,1:T(8,128)(2,1)S(1)}, u32[]{:S(2)}, u32[]{:S(2)}) async-start(bf16[128,4,256]{0,2,1:T(8,128)(2,1)} %bitcast.7), calls=%async_computation.1 | async-start | bytes 524288 | tf_op jit(solution)/shard_map/all_to_all | solution.py:78
  57.7 8.6 %copy-start.24 = (f32[512,4,64]{2,0,1:T(8,128)}, f32[512,4,64]{2,0,1:T(8,128)S(1)}, u32[]{:S(2)}) copy-start(f32[512,4,64]{2,0,1:T(8,128)S(1)} %copy.241) | copy-start | bytes 1572868
  77.6 38.5 %all-to-all-start.3 = ((bf16[128,4,256]{0,2,1:T(8,128)(2,1)}), bf16[128,4,256]{0,2,1:T(8,128)(2,1)S(1)}, u32[]{:S(2)}, u32[]{:S(2)}) async-start(bf16[128,4,256]{0,2,1:T(8,128)(2,1)} %bitcast.15), calls=%async_computation.3 | async-start | bytes 524288 | tf_op jit(solution)/shard_map/all_to_all | solution.py:76
  116.1 40.1 %all-to-all-start.4 = ((bf16[128,4,256]{0,2,1:T(8,128)(2,1)}), bf16[128,4,256]{0,2,1:T(8,128)(2,1)S(1)}, u32[]{:S(2)}, u32[]{:S(2)}) async-start(bf16[128,4,256]{0,2,1:T(8,128)(2,1)} %bitcast.194), calls=%async_computation.4 | async-start | bytes 524288 | tf_op jit(solution)/shard_map/all_to_all | solution.py:77
  156.2 18.7 %all-to-all-start = ((bf16[128,4,256]{0,2,1:T(8,128)(2,1)}), bf16[128,4,256]{0,2,1:T(8,128)(2,1)S(1)}, u32[]{:S(2)}, u32[]{:S(2)}) async-start(bf16[128,4,256]{0,2,1:T(8,128)(2,1)} %bitcast.193), calls=%async_computation | async-start | bytes 524288 | tf_op jit(solution)/shard_map/all_to_all | solution.py:75
  189.7 5.3 copy-start.34
  518.7 6.4 copy-start.29
  526.5 9.2 %copy-start.21 = (f32[512,4,64]{0,2,1:T(8,128)S(1)}, f32[512,4,64]{0,2,1:T(8,128)}, u32[]{:S(2)}) copy-start(f32[512,4,64]{0,2,1:T(8,128)} %reshape.199) | copy-start | bytes 1572868
  541.6 14.5 %copy-start.5 = (f32[1,8,64,4,64]{2,4,1,3,0:T(8,128)}, f32[1,8,64,4,64]{2,4,1,3,0:T(8,128)S(1)}, u32[]{:S(2)}) copy-start(f32[1,8,64,4,64]{2,4,1,3,0:T(8,128)S(1)} %copy.213) | copy-start | bytes 1572868
  543.4 12.7 %copy-start.7 = (f32[1,8,64,4,64]{2,4,1,3,0:T(8,128)}, f32[1,8,64,4,64]{2,4,1,3,0:T(8,128)S(1)}, u32[]{:S(2)}) copy-start(f32[1,8,64,4,64]{2,4,1,3,0:T(8,128)S(1)} %copy.212) | copy-start | bytes 1572868
  551.1 4.9 copy-start.3
  551.1 4.9 copy-start.11
  556.1 4.5 copy-start.26
  556.1 4.4 copy-start.27
  556.1 4.4 copy-start.33
  594.0 7.5 %copy-start.28 = (f32[512,4,64]{0,2,1:T(8,128)S(1)}, f32[512,4,64]{0,2,1:T(8,128)}, u32[]{:S(2)}) copy-start(f32[512,4,64]{0,2,1:T(8,128)} %rev.19) | copy-start | bytes 1572868
  605.4 8.1 %copy-start.9 = (f32[512,4,64]{2,0,1:T(8,128)S(1)}, f32[512,4,64]{2,0,1:T(8,128)}, u32[]{:S(2)}) copy-start(f32[512,4,64]{2,0,1:T(8,128)} %copy.238) | copy-start | bytes 1572868
  605.4 8.1 %copy-start.10 = (f32[1,8,64,4,64]{4,2,1,3,0:T(8,128)S(1)}, f32[1,8,64,4,64]{4,2,1,3,0:T(8,128)}, u32[]{:S(2)}) copy-start(f32[1,8,64,4,64]{4,2,1,3,0:T(8,128)} %copy.188) | copy-start | bytes 1572868
  605.4 8.1 %copy-start.31 = (f32[8,2,4,64,64]{3,4,2,1,0:T(8,128)S(1)}, f32[8,2,4,64,64]{3,4,2,1,0:T(8,128)}, u32[]{:S(2)}) copy-start(f32[8,2,4,64,64]{3,4,2,1,0:T(8,128)} %get-tuple-element.32) | copy-start | bytes 3145732
  617.5 6.0 copy-start.22
  624.9 5.2 copy-start.18
  646.8 16.9 %copy-start.1 = (bf16[1,128,2048]{2,1,0:T(8,128)(2,1)S(1)}, bf16[1,128,2048]{2,1,0:T(8,128)(2,1)}, u32[]{:S(2)}) copy-start(bf16[1,128,2048]{2,1,0:T(8,128)(2,1)} %param.12) | copy-start | bytes 1572868
  (15 other events, 42.7 us)
Sparse Core Ops, SparseCore 0:
  9.2 26.0 all-gather.6
  37.2 36.5 all-gather.8
  75.7 36.5 all-gather.10
  114.1 36.5 all-gather.4
where the time goes:
time: 678 us; the launch traced here: 671 us
  other arithmetic  335 us (49%)
  matrix products  106 us (16%)
  waiting for transfers between devices  105 us (15%)
  local copies, waits for them, and re-layouts  74.2 us (11%)
  starting transfers between devices  22.1 us (3%)
  between operations  14.2 us (2%)
  blocking collectives  13.6 us (2%)
    another operation x4, other arithmetic, per_device(): lax.linalg.triangular_solve(identity - erase_write, jnp.broadcast_to(iden...  317 us
    dot_general x22, matrix products, contract(): return jnp.einsum(pattern, former, latter, precision=lax.Precision.HIGHEST)  88.5 us
    all_gather x1, waiting for transfers between devices, per_device(): lax.all_gather(receptance_weight, 'dp', axis=0, tiled=True)  30 us
    convert_element_type x18, local copies, waits for them, and re-layouts, by_head(): content_matrix_full.astype(jnp.float32)  29.6 us
    all_gather x1, waiting for transfers between devices, per_device(): lax.all_gather(value_projection_weight, 'dp', axis=0, tiled=True)  29.5 us
    all_gather x1, waiting for transfers between devices, per_device(): lax.all_gather(decay_down_weight, 'dp', axis=0, tiled=True)  25.1 us
    all_to_all x1, blocking collectives, per_device(): lax.all_to_all(mixed, 'sp', split_axis=0, concat_axis=1, tiled=True)  13.6 us
  transfers between devices with their start and end apart: 9, of which 6 were waited for; matrix products, arithmetic and copies ran while one was open for 6% of the time, Pallas kernels for 0%

commit v1 on v0

v1 whole, which is shorter than its diff:
```python
import functools
import math

import jax
import jax.numpy as jnp
from jax import lax
from jax.experimental import pallas as pl
from jax.experimental.pallas import tpu as pltpu
from jax.sharding import PartitionSpec as P

HEAD = 64
SPAN = 64
BF = jnp.bfloat16
F32 = jnp.float32
NT = (((1,), (1,)), ((), ()))
TN = (((0,), (0,)), ((), ()))


def mm(a, b):
    return jnp.dot(a, b, preferred_element_type=F32)


def split(x):
    hi = x.astype(BF)
    return hi, (x - hi.astype(F32)).astype(BF)


def iota(shape, axis):
    return lax.broadcasted_iota(jnp.int32, shape, axis)


def core_kernel(
    tok_ref, w_ref, up_ref, floor_ref, rate_ref, diag_ref, gain_ref, out_ref,
    eq_s, wp_s, qe_s, kend_s, cv_s, own_s, decay_s, diag_s, t_s, b_s, state_s, y_s,
):
    length, chans = out_ref.shape
    heads = chans // HEAD
    rank = up_ref.shape[1]
    rows = min(256, length)
    spans = rows // SPAN
    blocks = length // SPAN

    def head_ones():
        return (iota((chans, chans), 0) // HEAD == iota((chans, chans), 1) // HEAD).astype(BF)

    def head_sum(x, ones):
        hi, lo = split(x)
        return mm(hi, ones) + mm(lo, ones)

    @pl.loop(0, length // rows)
    def _(step):
        at = pl.ds(pl.multiple_of(step * rows, rows), rows)
        source = tok_ref[at, :]
        pr = mm(source, w_ref[:, :chans]).astype(BF).astype(F32)
        pk = mm(source, w_ref[:, chans : 2 * chans]).astype(BF).astype(F32)
        pv = mm(source, w_ref[:, 2 * chans : 3 * chans]).astype(BF).astype(F32)
        lowered = jnp.tanh(mm(source, w_ref[:, 3 * chans :])).astype(BF)
        ones = head_ones()
        norm2 = head_sum(pk * pk, ones) + 1.0
        inv = lax.rsqrt(norm2)
        scale = norm2 * inv
        normed = pk * inv
        cv_s[at, :] = scale * pv
        rates = jax.nn.sigmoid(rate_ref[...])
        both = jnp.sum(rates * diag_ref[...], axis=0, keepdims=True)
        own_s[at, :] = head_sum(pr * pk * both, ones) * pv
        ri = iota((rows, rows), 0)
        ci = iota((rows, rows), 1)
        same = ri // SPAN == ci // SPAN
        whole = same.astype(BF)
        for d in range(2):
            pre = (
                mm(lowered[:, d * rank : (d + 1) * rank], up_ref[d]) + floor_ref[d : d + 1, :]
            ).astype(BF).astype(F32)
            fall = -math.exp(-0.5) * jax.nn.sigmoid(pre)
            tri = jnp.logical_and(same, (ci <= ri) if d == 0 else (ci >= ri)).astype(BF)
            hi, lo = split(fall)
            inclusive = mm(tri, hi) + mm(tri, lo)
            final = mm(whole, hi) + mm(whole, lo)
            half = 0.5 * final
            grow = jnp.exp(inclusive - half)
            shrink = jnp.exp(half - inclusive)
            g = jnp.exp(half)
            e = -normed * (grow * jnp.exp(-fall))
            q = pr * grow
            w = normed * rates[d : d + 1, :] * shrink
            wp_s[d, at, :] = w.astype(BF)
            kend_s[d, at, :] = (w * g).astype(BF)
            eb, qb = e.astype(BF), q.astype(BF)
            eg, qg = (e * g).astype(BF), (q * g).astype(BF)
            g2 = g * g
            diag_s[d, at, :] = head_sum(pr * normed * rates[d : d + 1, :], ones)
            for s in range(spans):
                cut = slice(s * SPAN, (s + 1) * SPAN)
                base = pl.multiple_of((step * spans + s) * 2 * SPAN, 2 * SPAN)
                eq_s[d, pl.ds(base, SPAN), :] = eb[cut]
                eq_s[d, pl.ds(base + SPAN, SPAN), :] = qb[cut]
                qe_s[d, pl.ds(base, SPAN), :] = eg[cut]
                qe_s[d, pl.ds(base + SPAN, SPAN), :] = qg[cut]
                decay_s[d, pl.ds(pl.multiple_of((step * spans + s) * 8, 8), 8), :] = g2[
                    s * SPAN : s * SPAN + 8
                ]

    def spread(x, mask):
        x = x.astype(BF)
        if heads > 1:
            x = jnp.concatenate([x] * heads, axis=0)
        return x * mask

    group = 2 if blocks % 2 == 0 else 1

    @pl.loop(0, blocks // group)
    def _(step):
        mask = head_ones()
        ti = iota((SPAN, chans), 0)
        ji = iota((SPAN, chans), 1) % HEAD
        eye = (ti == ji).astype(F32)
        work = []
        for s in range(group):
            for d in range(2):
                block = step * group + s
                two = pl.ds(pl.multiple_of(block * 2 * SPAN, 2 * SPAN), 2 * SPAN)
                at = pl.ds(pl.multiple_of(block * SPAN, SPAN), SPAN)
                ab = lax.dot_general(
                    eq_s[d, two, :], spread(wp_s[d, at, :], mask), NT, preferred_element_type=F32
                )
                strict = (ti > ji) if d == 0 else (ti < ji)
                b_s[d, at, :] = jnp.where(strict, ab[SPAN:], 0.0).astype(BF)
                work.append((d, at, jnp.where(strict, ab[:SPAN], 0.0)))
        near = ti // 4 == ji // 4
        full = [a for _, _, a in work]
        base = [jnp.where(near, a, 0.0) for a in full]
        square = [mm(a.astype(BF), spread(a, mask)) for a in base]
        inverse = [eye + a for a in base]
        inverse = [t + mm(t.astype(BF), spread(a2, mask)) for t, a2 in zip(inverse, square)]
        size = 4
        while size < SPAN:
            far = jnp.logical_and(ti // (2 * size) == ji // (2 * size), ti // size != ji // size)
            first = [
                mm(t.astype(BF), spread(jnp.where(far, a, 0.0), mask))
                for t, a in zip(inverse, full)
            ]
            inverse = [t + mm(f.astype(BF), spread(t, mask)) for t, f in zip(inverse, first)]
            size *= 2
        for (d, at, _), t in zip(work, inverse):
            t_s[d, at, :] = (t - eye).astype(BF)

    state_s[...] = jnp.zeros_like(state_s)

    @pl.loop(0, blocks)
    def _(step):
        mask = head_ones()
        for d in range(2):
            block = step if d == 0 else blocks - 1 - step
            two = pl.ds(pl.multiple_of(block * 2 * SPAN, 2 * SPAN), 2 * SPAN)
            at = pl.ds(pl.multiple_of(block * SPAN, SPAN), SPAN)
            state = state_s[d]
            read = lax.dot_general(
                qe_s[d, two, :], state.astype(BF), NT, preferred_element_type=F32
            )
            x = cv_s[at, :] + read[:SPAN]
            exact = x + mm(t_s[d, at, :], spread(x, mask))
            a = exact.astype(BF)
            y_s[d, at, :] = read[SPAN:] + mm(b_s[d, at, :], spread(a, mask)) + diag_s[d, at, :] * exact
            decay = decay_s[d, pl.ds(pl.multiple_of(block * 8, 8), 8), :][:1]
            put = lax.dot_general(a, kend_s[d, at, :], TN, preferred_element_type=F32)
            state_s[d] = state * decay + put * mask.astype(F32)

    @pl.loop(0, length // rows)
    def _(step):
        at = pl.ds(pl.multiple_of(step * rows, rows), rows)
        ones = head_ones()
        total = own_s[at, :]
        for d in range(2):
            y = y_s[d, at, :]
            centred = y - head_sum(y, ones) * (1.0 / HEAD)
            variance = head_sum(centred * centred, ones) * (1.0 / HEAD)
            total = total + centred * lax.rsqrt(variance + 0.00064) * gain_ref[...]
        out_ref[at, :] = total.astype(BF)


def core_call(length, chans, interpret=False):
    vm = pltpu.VMEM
    both = lambda n, dt: vm((2, n, chans), dt)
    return pl.pallas_call(
        core_kernel,
        out_shape=jax.ShapeDtypeStruct((length, chans), BF),
        in_specs=[pl.BlockSpec(memory_space=vm)] * 7,
        out_specs=pl.BlockSpec(memory_space=vm),
        scratch_shapes=[
            both(2 * length, BF), both(length, BF), both(2 * length, BF), both(length, BF),
            vm((length, chans), F32), vm((length, chans), F32),
            both(length // SPAN * 8, F32), both(length, F32), both(length, BF), both(length, BF),
            vm((2, chans, chans), F32), both(length, F32),
        ],
        compiler_params=pltpu.CompilerParams(vmem_limit_bytes=56 * 1024 * 1024),
        interpret=interpret,
        name="core",
    )


def per_device(
    sp,
    tokens, receptance_weight, key_projection_weight, value_projection_weight,
    decay_down_weight, decay_up_weight, decay_floor_level, correction_rate_logit,
    diagonal_address_factor, head_norm_gain,
):
    rows, depth = tokens.shape[1:]
    channels = receptance_weight.shape[1]
    chans = channels // sp
    start = lax.axis_index("sp") * chans

    def mine(x):
        return lax.dynamic_slice_in_dim(x, start, chans, axis=x.ndim - 1)

    packed = jnp.concatenate(
        [mine(receptance_weight), mine(key_projection_weight), mine(value_projection_weight),
         decay_down_weight], axis=1)
    weights = lax.all_gather(packed, "dp", axis=0, tiled=True)
    source = lax.all_gather(tokens[0], "sp", axis=0, tiled=True)
    mixed = core_call(rows * sp, chans)(
        source, weights, mine(decay_up_weight), mine(decay_floor_level),
        correction_rate_logit, diagonal_address_factor, head_norm_gain[None, :])
    returned = lax.all_to_all(mixed, "sp", split_axis=0, concat_axis=1, tiled=True)
    return returned[None]


def solution(mesh):
    in_specs = (
        P("dp", "sp", None), P("dp", None), P("dp", None), P("dp", None), P("dp", None),
        P(), P(), P(None, "sp"), P(None, "sp"), P("sp"),
    )
    return jax.shard_map(
        functools.partial(per_device, mesh.shape["sp"]), mesh=mesh, in_specs=in_specs,
        out_specs=P("dp", "sp", None), check_vma=False,
    )
```

time: 678 us -> 141 us (0.21); the launches traced: 671 us -> 141 us
  other arithmetic: 335 us -> 1.79 us
  matrix products: 106 us -> 0 us
  local copies, waits for them, and re-layouts: 74.2 us -> 5.21 us
  Pallas kernels: 0 us -> 24.1 us
  waiting for transfers between devices: 105 us -> 82.1 us
  starting transfers between devices: 22.1 us -> 0.04 us
    another operation x5 -> x0, other arithmetic: 318 us -> none  [the longest x4 317 us: per_device(): lax.linalg.triangular_solve(identity - erase_write, jnp.broadcast_to(iden...]
    dot_general x28 -> x0, matrix products: 99.9 us -> none  [the longest x22 88.5 us: contract(): return jnp.einsum(pattern, former, latter, precision=lax.Precision.HIGHEST)]
    convert_element_type x20 -> x0, local copies, waits for them, and re-layouts: 29.7 us -> none  [the longest x18 29.6 us: by_head(): content_matrix_full.astype(jnp.float32)]
    pallas_call x0 -> x1, Pallas kernels: none -> 24.1 us  [per_device(): core_call(rows * sp, chans)]
    all_to_all x5 -> x0, starting transfers between devices: 22 us -> none  [the longest x1 4.78 us: per_device(): lax.all_to_all(receive, 'sp', split_axis=1, concat_axis=0, tiled=True)]
    rev x6 -> x0, local copies, waits for them, and re-layouts: 16.6 us -> none  [the longest x4 9.31 us: both_ways(): return jnp.stack([content_matrix_full, jnp.flip(content_matrix_full, 0)], 0)]
    all_to_all x5 -> x0, waiting for transfers between devices: 12.8 us -> none  [the longest x1 8.21 us: per_device(): lax.all_to_all(backward_pre, 'sp', split_axis=1, concat_axis=0, tiled=True)]
    another operation x6 -> x0, local copies, waits for them, and re-layouts: 8.12 us -> none  [the longest x5 7.79 us: both_ways(): return jnp.stack([content_matrix_full, jnp.flip(content_matrix_full, 0)], 0)]
  transfers between devices with their start and end apart: 9 -> 2, of which waited for: 6 -> 2; matrix products, arithmetic and copies ran while one was open for 6% -> 4% of each run, Pallas kernels for 0% -> 0%
where the time goes in v1:
time: 141 us
  waiting for transfers between devices  82.1 us (58%)
  Pallas kernels  24.1 us (17%)
  blocking collectives  13.9 us (10%)
  between operations  13.4 us (10%)
  local copies, waits for them, and re-layouts  5.21 us (4%)
  other arithmetic  1.79 us (1%)
    all_gather x1, waiting for transfers between devices, per_device(): source = lax.all_gather(tokens[0], 'sp', axis=0, tiled=True)  44.1 us
    all_gather x1, waiting for transfers between devices, per_device(): weights = lax.all_gather(packed, 'dp', axis=0, tiled=True)  37.3 us
    pallas_call x1, Pallas kernels, per_device(): core_call(rows * sp, chans)  24.1 us
    all_to_all x1, blocking collectives, per_device(): lax.all_to_all(mixed, 'sp', split_axis=0, concat_axis=1, tiled=True)  13.9 us
    dynamic_slice x4, local copies, waits for them, and re-layouts, mine(): return lax.dynamic_slice_in_dim(x, start, chans, axis=x.ndim - 1)  3.86 us
  transfers between devices with their start and end apart: 2, of which 2 were waited for; matrix products, arithmetic and copies ran while one was open for 4% of the time, Pallas kernels for 0%

profile of v1, /device:TPU:0, one launch (start us, length us, event | category | flops | bytes accessed | tf_op | source)
XLA Modules:
  0.0 140.5 jit_solution(11929086850064901882)
XLA Ops:
  6.5 0.0 copy-start
  6.5 0.0 all-gather.6.cloned.1.call-start
  6.5 0.7 all-gather.6.cloned.1.call-update
  7.3 0.0 all-gather.4.cloned.1.call-start
  7.3 0.3 copy-done
  7.6 1.0 constant_dynamic-slice_fusion.2
  8.6 1.8 %pad_maximum_fusion = bf16[256,1024]{1,0:T(8,128)(2,1)} fusion(bf16[256,256]{1,0:T(8,128)(2,1)} %param.14, bf16[256,256]{1,0:T(8,128)(2,1)S(1)} %get-tuple-element.5, bf16[256,256]{1,0:T(8,128)(2,1)S(1)} %get-tuple-element.6, bf16[256,256]{1,0:T(8,128)(2,1)S(1)} %constant_dynamic-slice_fusion.4), kind=kLoop, calls=%fused_computation | loop fusion | flops 2097152 | bytes 1048576 | tf_op jit(solution)/shard_map/concatenate | solution.py:216
  10.4 0.0 all-gather.4.cloned.1.call-update
  10.4 1.3 constant_dynamic-slice_fusion.floor_ref
  11.7 1.6 %constant_dynamic-slice_fusion.1.up_ref = bf16[2,128,256]{2,1,0:T(8,128)(2,1)} fusion(bf16[2,128,1024]{2,1,0:T(8,128)(2,1)} %param.15, s32[]{:T(128)S(6)} %select_n.2), kind=kLoop, calls=%fused_computation.2 | loop fusion | bytes 262148 | tf_op jit(solution)/shard_map/dynamic_slice | solution.py:214
  13.3 44.1 %all-gather.6.cloned.1.call-done = bf16[1,512,2048]{2,1,0:T(8,128)(2,1)} async-done(((bf16[1,128,2048]{2,1,0:T(8,128)(2,1)}), bf16[1,512,2048]{2,1,0:T(8,128)(2,1)}) %all-gather.6.cloned.1.call-update) | async-done | bytes 2097168 | tf_op jit(solution)/shard_map/all_gather | solution.py:220
  57.3 37.3 %all-gather.4.cloned.1.call-done.w_ref = bf16[2048,1024]{1,0:T(8,128)(2,1)} async-done(((bf16[256,1024]{1,0:T(8,128)(2,1)}), bf16[2048,1024]{1,0:T(8,128)(2,1)}) %all-gather.4.cloned.1.call-update) | async-done | bytes 4194320 | tf_op jit(solution)/shard_map/all_gather | solution.py:219
  94.6 24.1 %core.1 = bf16[512,256]{1,0:T(8,128)(2,1)} custom-call(bf16[512,2048]{1,0:T(8,128)(2,1)} %bitcast.4, bf16[2048,1024]{1,0:T(8,128)(2,1)} %all-gather.4.cloned.1.call-done.w_ref, bf16[2,128,256]{2,1,0:T(8,128)(2,1)} %constant_dynamic-slice_fusion.1.up_ref, f32[2,256]{1,0:T(2,128)} %constant_dynamic-slice_fusion.floor_ref, f32[2,256]{1,0:T(2,128)} %rate_ref.1, ...), custom_call_target="tpu_custom_call" | custom-call | tf_op jit(solution)/shard_map/core/pallas_call | solution.py:221
  118.7 13.9 %all_to_all.16 = bf16[4,128,256]{2,1,0:T(8,128)(2,1)S(1)} all-to-all(bf16[4,128,256]{2,1,0:T(8,128)(2,1)} %bitcast.5), channel_id=1, replica_groups=mesh['sp'=4,'dp'=8] {'sp'}, dimensions={0} | all-to-all | bytes 524288 | tf_op jit(solution)/shard_map/all_to_all | solution.py:224
  132.6 0.2 copy.11
  132.8 0.9 broadcast_in_dim.7
  (1 shorter events, 0.0 us)
Async XLA Ops:
  6.5 1.0 copy-start
  6.5 50.8 %all-gather.6.cloned.1.call-start = ((), (), s32[]{:S(2)}) async-start(), calls=%async_computation.2 | async-start | bytes 2621440 | tf_op jit(solution)/shard_map/all_gather | solution.py:220
  7.3 87.4 %all-gather.4.cloned.1.call-start = ((), (), s32[]{:S(2)}) async-start(), calls=%async_computation.1 | async-start | bytes 4718592 | tf_op jit(solution)/shard_map/all_gather | solution.py:219
Sparse Core Ops, SparseCore 0:
  8.9 48.3 all-gather.5
  59.2 35.3 all-gather.3

commit v2 on v1

--- a/solution.py
+++ b/solution.py
@@ -179,28 +179,144 @@
         out_ref[at, :] = total.astype(BF)
 
 
-def core_call(length, chans, interpret=False):
+MESH = pl.DeviceIdType.MESH
+
+
+def whole_kernel(
+    sp, dp, tok_ref, w_ref, up_ref, floor_ref, rate_ref, diag_ref, gain_ref, out_ref,
+    tok_all, w_all, out_all, slots,
+    ring_out, ring_in, far_out, far_in, pass_out, pass_in, back_out, back_in, *scratch,
+):
+    rows = tok_ref.shape[0]
+    half_rows = rows // 2
+    depth = w_ref.shape[0]
+    chans = out_all.shape[1]
+    chips = dp // 2
+    z = lax.axis_index("sp")
+    me = lax.axis_index("dp")
+    chip = me // 2
+    core = me % 2
+    partner = chip * 2 + 1 - core
+
+    def peer(k):
+        return lax.rem(chip + k, chips) * 2 + core
+
+    def z_peer(k):
+        return lax.rem(z + k, sp)
+
+    barrier = pltpu.get_barrier_semaphore()
+    for target in [(z, partner)] + [(z, peer(k)) for k in range(1, chips)] + [
+        (z_peer(k), me) for k in range(1, sp)
+    ]:
+        pl.semaphore_signal(barrier, inc=1, device_id=target, device_id_type=MESH)
+    pl.semaphore_wait(barrier, chips + sp - 1)
+
+    def remote(src, dst, out_sem, in_sem, target):
+        copy = pltpu.make_async_remote_copy(
+            src_ref=src, dst_ref=dst, send_sem=out_sem, recv_sem=in_sem,
+            device_id=target, device_id_type=MESH,
+        )
+        copy.start()
+        return copy
+
+    def w_at(device):
+        return pl.ds(pl.multiple_of(device * depth, depth), depth)
+
+    def ring_step(s):
+        copies = []
+        for way in range(2):
+            owner = z_peer(sp - s) if way == 0 else z_peer(s)
+            at = pl.ds(
+                pl.multiple_of(owner * rows + way * half_rows, half_rows), half_rows
+            )
+            first = tok_ref.at[pl.ds(way * half_rows, half_rows), :]
+            copies.append(
+                remote(
+                    first if s == 0 else tok_all.at[at, :], tok_all.at[at, :],
+                    ring_out.at[way, s], ring_in.at[way, s],
+                    (z_peer(1) if way == 0 else z_peer(sp - 1), me),
+                )
+            )
+        return copies
+
+    ring = [ring_step(0)] if sp > 1 else []
+    far = [
+        remote(w_ref, w_all.at[w_at(me), :], far_out.at[k], far_in.at[k], (z, peer(k)))
+        for k in range(1, chips)
+    ]
+    passed = [remote(w_ref, w_all.at[w_at(me), :], pass_out.at[0], pass_in.at[0], (z, partner))]
+    w_all[w_at(me), :] = w_ref[...]
+    tok_all[pl.ds(pl.multiple_of(z * rows, rows), rows), :] = tok_ref[...]
+    for s in range(max(sp, chips) - 1):
+        if s < sp - 1:
+            for copy in ring[s]:
+                copy.wait_recv()
+            if s + 1 < sp - 1:
+                ring.append(ring_step(s + 1))
+        if s < chips - 1:
+            far[s].wait_recv()
+            block = w_at(peer(chips - 1 - s))
+            passed.append(
+                remote(
+                    w_all.at[block, :], w_all.at[block, :],
+                    pass_out.at[s + 1], pass_in.at[s + 1], (z, partner),
+                )
+            )
+    for copy in passed:
+        copy.wait_recv()
+    for copy in far + passed + [c for pair in ring for c in pair]:
+        copy.wait_send()
+
+    core_kernel(
+        tok_all, w_all, up_ref, floor_ref, rate_ref, diag_ref, gain_ref, out_all, *scratch
+    )
+
+    def out_at(owner):
+        return pl.ds(pl.multiple_of(owner * rows, rows), rows)
+
+    back = [
+        remote(
+            out_all.at[out_at(z_peer(k)), :], slots.at[z], back_out.at[k], back_in.at[k],
+            (z_peer(k), me),
+        )
+        for k in range(1, sp)
+    ]
+    slots[z] = out_all[out_at(z), :]
+    for copy in back:
+        copy.wait()
+    for s in range(sp):
+        out_ref[:, s * chans : (s + 1) * chans] = slots[s]
+
+
+def whole_call(sp, dp, rows, depth, chans, width):
     vm = pltpu.VMEM
+    dma = pltpu.SemaphoreType.DMA
+    length = rows * sp
     both = lambda n, dt: vm((2, n, chans), dt)
     return pl.pallas_call(
-        core_kernel,
-        out_shape=jax.ShapeDtypeStruct((length, chans), BF),
+        functools.partial(whole_kernel, sp, dp),
+        out_shape=jax.ShapeDtypeStruct((rows, chans * sp), BF),
         in_specs=[pl.BlockSpec(memory_space=vm)] * 7,
         out_specs=pl.BlockSpec(memory_space=vm),
         scratch_shapes=[
+            vm((length, depth), BF), vm((depth, width), BF), vm((length, chans), BF),
+            vm((sp, rows, chans), BF),
+            dma((2, sp)), dma((2, sp)), dma((dp,)), dma((dp,)), dma((dp,)), dma((dp,)),
+            dma((sp,)), dma((sp,)),
             both(2 * length, BF), both(length, BF), both(2 * length, BF), both(length, BF),
             vm((length, chans), F32), vm((length, chans), F32),
             both(length // SPAN * 8, F32), both(length, F32), both(length, BF), both(length, BF),
             vm((2, chans, chans), F32), both(length, F32),
         ],
-        compiler_params=pltpu.CompilerParams(vmem_limit_bytes=56 * 1024 * 1024),
-        interpret=interpret,
-        name="core",
+        compiler_params=pltpu.CompilerParams(
+            vmem_limit_bytes=58 * 1024 * 1024, collective_id=0, has_side_effects=True
+        ),
+        name="whole",
     )
 
 
 def per_device(
-    sp,
+    sp, dp,
     tokens, receptance_weight, key_projection_weight, value_projection_weight,
     decay_down_weight, decay_up_weight, decay_floor_level, correction_rate_logit,
     diagonal_address_factor, head_norm_gain,
@@ -216,13 +332,10 @@
     packed = jnp.concatenate(
         [mine(receptance_weight), mine(key_projection_weight), mine(value_projection_weight),
          decay_down_weight], axis=1)
-    weights = lax.all_gather(packed, "dp", axis=0, tiled=True)
-    source = lax.all_gather(tokens[0], "sp", axis=0, tiled=True)
-    mixed = core_call(rows * sp, chans)(
-        source, weights, mine(decay_up_weight), mine(decay_floor_level),
+    mixed = whole_call(sp, dp, rows, depth, chans, packed.shape[1])(
+        tokens[0], packed, mine(decay_up_weight), mine(decay_floor_level),
         correction_rate_logit, diagonal_address_factor, head_norm_gain[None, :])
-    returned = lax.all_to_all(mixed, "sp", split_axis=0, concat_axis=1, tiled=True)
-    return returned[None]
+    return mixed[None]
 
 
 def solution(mesh):
@@ -231,6 +344,6 @@
         P(), P(), P(None, "sp"), P(None, "sp"), P("sp"),
     )
     return jax.shard_map(
-        functools.partial(per_device, mesh.shape["sp"]), mesh=mesh, in_specs=in_specs,
+        functools.partial(per_device, mesh.shape["sp"], mesh.shape["dp"]), mesh=mesh, in_specs=in_specs,
         out_specs=P("dp", "sp", None), check_vma=False,
     )

time: 141 us -> 81.9 us (0.58)
  waiting for transfers between devices: 82.1 us -> 0 us
  Pallas kernels: 24.1 us -> 74.2 us
  blocking collectives: 13.9 us -> 0 us
  between operations: 13.4 us -> 0.02 us
    all_gather x2 -> x0, waiting for transfers between devices: 81.4 us -> none  [the longest x1 44.1 us: per_device(): source = lax.all_gather(tokens[0], 'sp', axis=0, tiled=True)]
    pallas_call x1, Pallas kernels: 24.1 us -> 74.2 us  [per_device(): whole_call(sp, dp, rows, depth, chans, packed.shape[1])]
    all_to_all x1 -> x0, blocking collectives: 13.9 us -> none  [per_device(): lax.all_to_all(mixed, 'sp', split_axis=0, concat_axis=1, tiled=True)]
    unnamed x2 -> x5, local copies, waits for them, and re-layouts: 0.27 us -> 2.68 us
  transfers between devices with their start and end apart: 2 -> 0, of which waited for: 2 -> 0; matrix products, arithmetic and copies ran while one was open for 4% -> 0% of each run, Pallas kernels for 0% -> 0%
where the time goes in v2:
time: 81.9 us; the launch traced here: 81.7 us
  Pallas kernels  74.2 us (91%)
  local copies, waits for them, and re-layouts  6.56 us (8%)
  other arithmetic  0.86 us (1%)
    pallas_call x1, Pallas kernels, per_device(): whole_call(sp, dp, rows, depth, chans, packed.shape[1])  74.2 us
    dynamic_slice x4, local copies, waits for them, and re-layouts, mine(): return lax.dynamic_slice_in_dim(x, start, chans, axis=x.ndim - 1)  3.89 us
    unnamed x5, local copies, waits for them, and re-layouts  2.68 us

profile of v2, /device:TPU:0, one launch (start us, length us, event | category | flops | bytes accessed | tf_op | source)
XLA Modules:
  0.0 81.7 jit_solution(5704945131664997151)
XLA Ops:
  0.0 0.0 copy-start
  0.0 1.0 %constant_dynamic-slice_fusion.2 = (bf16[256,256]{1,0:T(8,128)(2,1)S(1)}, bf16[256,256]{1,0:T(8,128)(2,1)S(1)}) fusion(bf16[256,1024]{1,0:T(8,128)(2,1)} %param.13, s32[]{:T(128)S(6)} %select_n.2, bf16[256,1024]{1,0:T(8,128)(2,1)} %param.12), kind=kLoop, calls=%fused_computation.3 | loop fusion | bytes 524292 | tf_op jit(solution)/shard_map/dynamic_slice | solution.py:330
  1.1 0.1 copy-done
  1.2 0.0 copy-start.1
  1.2 0.9 %copy-done.1 = bf16[256,256]{1,0:T(8,128)(2,1)S(1)} copy-done((bf16[256,256]{1,0:T(8,128)(2,1)S(1)}, bf16[256,256]{1,0:T(8,128)(2,1)}, u32[]{:S(2)}) %copy-start.1) | copy-done | bytes 131096
  2.1 0.9 %pad_maximum_fusion.w_ref = bf16[256,1024]{1,0:T(8,128)(2,1)} fusion(bf16[256,256]{1,0:T(8,128)(2,1)S(1)} %copy-done.1, bf16[256,256]{1,0:T(8,128)(2,1)S(1)} %get-tuple-element.5, bf16[256,256]{1,0:T(8,128)(2,1)S(1)} %get-tuple-element.6, bf16[256,256]{1,0:T(8,128)(2,1)S(1)} %constant_dynamic-slice_fusion.4), kind=kLoop, calls=%fused_computation | loop fusion | flops 2097152 | bytes 1048576 | tf_op jit(solution)/shard_map/concatenate | solution.py:332
  2.9 1.6 %constant_dynamic-slice_fusion.1.up_ref = bf16[2,128,256]{2,1,0:T(8,128)(2,1)} fusion(bf16[2,128,1024]{2,1,0:T(8,128)(2,1)} %param.15, s32[]{:T(128)S(6)} %select_n.2), kind=kLoop, calls=%fused_computation.2 | loop fusion | bytes 262148 | tf_op jit(solution)/shard_map/dynamic_slice | solution.py:330
  4.5 1.3 %constant_dynamic-slice_fusion.floor_ref = f32[2,256]{1,0:T(2,128)} fusion(f32[2,1024]{1,0:T(2,128)} %param.16, s32[]{:T(128)S(6)} %select_n.2), kind=kLoop, calls=%fused_computation.1 | loop fusion | bytes 4100 | tf_op jit(solution)/shard_map/dynamic_slice | solution.py:330
  5.8 74.2 %whole.1 = bf16[128,1024]{1,0:T(8,128)(2,1)} custom-call(bf16[128,2048]{1,0:T(8,128)(2,1)} %bitcast.4, bf16[256,1024]{1,0:T(8,128)(2,1)} %pad_maximum_fusion.w_ref, bf16[2,128,256]{2,1,0:T(8,128)(2,1)} %constant_dynamic-slice_fusion.1.up_ref, f32[2,256]{1,0:T(2,128)} %constant_dynamic-slice_fusion.floor_ref, f32[2,256]{1,0:T(2,128)} %rate_ref.1, ...), custom_call_target="tpu_custom_call" | custom-call | tf_op jit(solution)/shard_map/whole/pallas_call | solution.py:335
  80.0 1.7 %copy.12 = bf16[1,128,1024]{2,1,0:T(8,128)(2,1)} copy(bf16[1,128,1024]{2,1,0:T(8,128)(2,1)} %bitcast.3) | data formatting | bytes 524288
  (1 shorter events, 0.0 us)
Async XLA Ops:
  0.0 1.2 %copy-start = (bf16[256,1024]{1,0:T(8,128)(2,1)S(1)}, bf16[256,1024]{1,0:T(8,128)(2,1)}, u32[]{:S(2)}) copy-start(bf16[256,1024]{1,0:T(8,128)(2,1)} %param.11) | copy-start | bytes 1572868
  1.2 0.9 %copy-start.1 = (bf16[256,256]{1,0:T(8,128)(2,1)S(1)}, bf16[256,256]{1,0:T(8,128)(2,1)}, u32[]{:S(2)}) copy-start(bf16[256,256]{1,0:T(8,128)(2,1)} %param.14) | copy-start | bytes 393220

commit v3 on v2

--- a/solution.py
+++ b/solution.py
@@ -32,12 +32,12 @@
 def core_kernel(
     tok_ref, w_ref, up_ref, floor_ref, rate_ref, diag_ref, gain_ref, out_ref,
     eq_s, wp_s, qe_s, kend_s, cv_s, own_s, decay_s, diag_s, t_s, b_s, state_s, y_s,
+    arrivals=(),
 ):
     length, chans = out_ref.shape
     heads = chans // HEAD
     rank = up_ref.shape[1]
     rows = min(256, length)
-    spans = rows // SPAN
     blocks = length // SPAN
 
     def head_ones():
@@ -47,10 +47,17 @@
         hi, lo = split(x)
         return mm(hi, ones) + mm(lo, ones)
 
-    @pl.loop(0, length // rows)
-    def _(step):
-        at = pl.ds(pl.multiple_of(step * rows, rows), rows)
-        source = tok_ref[at, :]
+    def at_block(block):
+        return pl.ds(pl.multiple_of(block * SPAN, SPAN), SPAN)
+
+    def project(ready):
+        tile = SPAN * len(ready)
+
+        def put(ref, x, *lead):
+            for s, block in enumerate(ready):
+                ref[(*lead, at_block(block), slice(None))] = x[s * SPAN : (s + 1) * SPAN]
+
+        source = jnp.concatenate([tok_ref[at_block(block), :] for block in ready], axis=0)
         pr = mm(source, w_ref[:, :chans]).astype(BF).astype(F32)
         pk = mm(source, w_ref[:, chans : 2 * chans]).astype(BF).astype(F32)
         pv = mm(source, w_ref[:, 2 * chans : 3 * chans]).astype(BF).astype(F32)
@@ -60,12 +67,12 @@
         inv = lax.rsqrt(norm2)
         scale = norm2 * inv
         normed = pk * inv
-        cv_s[at, :] = scale * pv
+        put(cv_s, scale * pv)
         rates = jax.nn.sigmoid(rate_ref[...])
         both = jnp.sum(rates * diag_ref[...], axis=0, keepdims=True)
-        own_s[at, :] = head_sum(pr * pk * both, ones) * pv
-        ri = iota((rows, rows), 0)
-        ci = iota((rows, rows), 1)
+        put(own_s, head_sum(pr * pk * both, ones) * pv)
+        ri = iota((tile, tile), 0)
+        ci = iota((tile, tile), 1)
         same = ri // SPAN == ci // SPAN
         whole = same.astype(BF)
         for d in range(2):
@@ -84,20 +91,20 @@
             e = -normed * (grow * jnp.exp(-fall))
             q = pr * grow
             w = normed * rates[d : d + 1, :] * shrink
-            wp_s[d, at, :] = w.astype(BF)
-            kend_s[d, at, :] = (w * g).astype(BF)
+            put(wp_s, w.astype(BF), d)
+            put(kend_s, (w * g).astype(BF), d)
             eb, qb = e.astype(BF), q.astype(BF)
             eg, qg = (e * g).astype(BF), (q * g).astype(BF)
             g2 = g * g
-            diag_s[d, at, :] = head_sum(pr * normed * rates[d : d + 1, :], ones)
-            for s in range(spans):
+            put(diag_s, head_sum(pr * normed * rates[d : d + 1, :], ones), d)
+            for s, block in enumerate(ready):
                 cut = slice(s * SPAN, (s + 1) * SPAN)
-                base = pl.multiple_of((step * spans + s) * 2 * SPAN, 2 * SPAN)
+                base = pl.multiple_of(block * 2 * SPAN, 2 * SPAN)
                 eq_s[d, pl.ds(base, SPAN), :] = eb[cut]
                 eq_s[d, pl.ds(base + SPAN, SPAN), :] = qb[cut]
                 qe_s[d, pl.ds(base, SPAN), :] = eg[cut]
                 qe_s[d, pl.ds(base + SPAN, SPAN), :] = qg[cut]
-                decay_s[d, pl.ds(pl.multiple_of((step * spans + s) * 8, 8), 8), :] = g2[
+                decay_s[d, pl.ds(pl.multiple_of(block * 8, 8), 8), :] = g2[
                     s * SPAN : s * SPAN + 8
                 ]
 
@@ -107,18 +114,14 @@
             x = jnp.concatenate([x] * heads, axis=0)
         return x * mask
 
-    group = 2 if blocks % 2 == 0 else 1
-
-    @pl.loop(0, blocks // group)
-    def _(step):
+    def invert(ready):
         mask = head_ones()
         ti = iota((SPAN, chans), 0)
         ji = iota((SPAN, chans), 1) % HEAD
         eye = (ti == ji).astype(F32)
         work = []
-        for s in range(group):
+        for block in ready:
             for d in range(2):
-                block = step * group + s
                 two = pl.ds(pl.multiple_of(block * 2 * SPAN, 2 * SPAN), 2 * SPAN)
                 at = pl.ds(pl.multiple_of(block * SPAN, SPAN), SPAN)
                 ab = lax.dot_general(
@@ -145,6 +148,11 @@
         for (d, at, _), t in zip(work, inverse):
             t_s[d, at, :] = (t - eye).astype(BF)
 
+    for settle, ready in arrivals:
+        settle()
+        project(ready)
+        invert(ready)
+
     state_s[...] = jnp.zeros_like(state_s)
 
     @pl.loop(0, blocks)
@@ -248,11 +256,10 @@
     w_all[w_at(me), :] = w_ref[...]
     tok_all[pl.ds(pl.multiple_of(z * rows, rows), rows), :] = tok_ref[...]
     for s in range(max(sp, chips) - 1):
-        if s < sp - 1:
+        if s < sp - 2:
             for copy in ring[s]:
                 copy.wait_recv()
-            if s + 1 < sp - 1:
-                ring.append(ring_step(s + 1))
+            ring.append(ring_step(s + 1))
         if s < chips - 1:
             far[s].wait_recv()
             block = w_at(peer(chips - 1 - s))
@@ -264,12 +271,25 @@
             )
     for copy in passed:
         copy.wait_recv()
+
+    def last_ring():
+        for copy in ring[-1]:
+            copy.wait_recv()
+
+    per = rows // SPAN
+    arrivals = [(lambda: None, [z * per + b for b in range(per)])]
+    for s in range(sp - 1):
+        before, after = z_peer(sp - 1 - s), z_peer(s + 1)
+        ready = [before * per + b for b in range(per // 2)]
+        ready += [after * per + b for b in range(per // 2, per)]
+        arrivals.append((last_ring if s == sp - 2 else lambda: None, ready))
+
+    core_kernel(
+        tok_all, w_all, up_ref, floor_ref, rate_ref, diag_ref, gain_ref, out_all, *scratch,
+        arrivals=arrivals,
+    )
     for copy in far + passed + [c for pair in ring for c in pair]:
         copy.wait_send()
-
-    core_kernel(
-        tok_all, w_all, up_ref, floor_ref, rate_ref, diag_ref, gain_ref, out_all, *scratch
-    )
 
     def out_at(owner):
         return pl.ds(pl.multiple_of(owner * rows, rows), rows)

time: 81.9 us -> 71.5 us (0.87)
  Pallas kernels: 74.2 us -> 63.8 us
    pallas_call x1, Pallas kernels: 74.2 us -> 63.8 us  [per_device(): whole_call(sp, dp, rows, depth, chans, packed.shape[1])]
where the time goes in v3:
time: 71.5 us; the launch traced here: 71.2 us
  Pallas kernels  63.8 us (89%)
  local copies, waits for them, and re-layouts  6.56 us (9%)
  other arithmetic  0.86 us (1%)
    pallas_call x1, Pallas kernels, per_device(): whole_call(sp, dp, rows, depth, chans, packed.shape[1])  63.8 us
    dynamic_slice x4, local copies, waits for them, and re-layouts, mine(): return lax.dynamic_slice_in_dim(x, start, chans, axis=x.ndim - 1)  3.89 us
    unnamed x5, local copies, waits for them, and re-layouts  2.68 us

profile of v3, /device:TPU:0, one launch (start us, length us, event | category | flops | bytes accessed | tf_op | source)
XLA Modules:
  0.0 71.2 jit_solution(15353320635220030655)
XLA Ops:
  0.0 0.0 copy-start
  0.0 1.0 %constant_dynamic-slice_fusion.2 = (bf16[256,256]{1,0:T(8,128)(2,1)S(1)}, bf16[256,256]{1,0:T(8,128)(2,1)S(1)}) fusion(bf16[256,1024]{1,0:T(8,128)(2,1)} %param.13, s32[]{:T(128)S(6)} %select_n.2, bf16[256,1024]{1,0:T(8,128)(2,1)} %param.12), kind=kLoop, calls=%fused_computation.3 | loop fusion | bytes 524292 | tf_op jit(solution)/shard_map/dynamic_slice | solution.py:350
  1.1 0.1 copy-done
  1.2 0.0 copy-start.1
  1.2 0.9 %copy-done.1 = bf16[256,256]{1,0:T(8,128)(2,1)S(1)} copy-done((bf16[256,256]{1,0:T(8,128)(2,1)S(1)}, bf16[256,256]{1,0:T(8,128)(2,1)}, u32[]{:S(2)}) %copy-start.1) | copy-done | bytes 131096
  2.1 0.9 %pad_maximum_fusion.w_ref = bf16[256,1024]{1,0:T(8,128)(2,1)} fusion(bf16[256,256]{1,0:T(8,128)(2,1)S(1)} %copy-done.1, bf16[256,256]{1,0:T(8,128)(2,1)S(1)} %get-tuple-element.5, bf16[256,256]{1,0:T(8,128)(2,1)S(1)} %get-tuple-element.6, bf16[256,256]{1,0:T(8,128)(2,1)S(1)} %constant_dynamic-slice_fusion.4), kind=kLoop, calls=%fused_computation | loop fusion | flops 2097152 | bytes 1048576 | tf_op jit(solution)/shard_map/concatenate | solution.py:352
  2.9 1.6 %constant_dynamic-slice_fusion.1.up_ref = bf16[2,128,256]{2,1,0:T(8,128)(2,1)} fusion(bf16[2,128,1024]{2,1,0:T(8,128)(2,1)} %param.15, s32[]{:T(128)S(6)} %select_n.2), kind=kLoop, calls=%fused_computation.2 | loop fusion | bytes 262148 | tf_op jit(solution)/shard_map/dynamic_slice | solution.py:350
  4.5 1.3 %constant_dynamic-slice_fusion.floor_ref = f32[2,256]{1,0:T(2,128)} fusion(f32[2,1024]{1,0:T(2,128)} %param.16, s32[]{:T(128)S(6)} %select_n.2), kind=kLoop, calls=%fused_computation.1 | loop fusion | bytes 4100 | tf_op jit(solution)/shard_map/dynamic_slice | solution.py:350
  5.8 63.8 %whole.1 = bf16[128,1024]{1,0:T(8,128)(2,1)} custom-call(bf16[128,2048]{1,0:T(8,128)(2,1)} %bitcast.4, bf16[256,1024]{1,0:T(8,128)(2,1)} %pad_maximum_fusion.w_ref, bf16[2,128,256]{2,1,0:T(8,128)(2,1)} %constant_dynamic-slice_fusion.1.up_ref, f32[2,256]{1,0:T(2,128)} %constant_dynamic-slice_fusion.floor_ref, f32[2,256]{1,0:T(2,128)} %rate_ref.1, ...), custom_call_target="tpu_custom_call" | custom-call | tf_op jit(solution)/shard_map/whole/pallas_call | solution.py:355
  69.6 1.7 %copy.12 = bf16[1,128,1024]{2,1,0:T(8,128)(2,1)} copy(bf16[1,128,1024]{2,1,0:T(8,128)(2,1)} %bitcast.3) | data formatting | bytes 524288
  (1 shorter events, 0.0 us)
Async XLA Ops:
  0.0 1.2 %copy-start = (bf16[256,1024]{1,0:T(8,128)(2,1)S(1)}, bf16[256,1024]{1,0:T(8,128)(2,1)}, u32[]{:S(2)}) copy-start(bf16[256,1024]{1,0:T(8,128)(2,1)} %param.11) | copy-start | bytes 1572868
  1.2 0.9 %copy-start.1 = (bf16[256,256]{1,0:T(8,128)(2,1)S(1)}, bf16[256,256]{1,0:T(8,128)(2,1)}, u32[]{:S(2)}) copy-start(bf16[256,256]{1,0:T(8,128)(2,1)} %param.14) | copy-start | bytes 393220
